TPU v7x, 256 devices: a whole 4x4x8 slice. The times are simulated.
256 devices in a mesh: sp: 32 (over z, y), tp: 8 (over x, core).
Axes of the slice: x: 4, y: 4, z: 8, core: 2. Of those that a mesh axis runs over, the one named last changes fastest.
Arguments:
- latents: bfloat16 [10240, 2048], P(('sp', 'tp')), may hold values from -12.5 to 12.5, as said below
- context: bfloat16 [1024, 2048], P('sp'), may hold values from -120 to 120, as said below
- cond_vec: float32 [2048], replicated, may hold values from -6 to 6
- ctx_vec: float32 [2048], replicated, may hold values from -6 to 6
- shift_w: bfloat16 [2048, 2048], P('sp', 'tp'), may hold values from -0.125 to 0.125
- scale_w: bfloat16 [2048, 2048], P('sp', 'tp'), may hold values from -0.125 to 0.125
- modgate_w: bfloat16 [2048, 2048], P('sp', 'tp'), may hold values from -0.125 to 0.125
- query_down_weight: bfloat16 [2048, 512], replicated, may hold values from -0.125 to 0.125
- latent_down_weight: bfloat16 [2048, 256], replicated, may hold values from -0.125 to 0.125
- rot_down: bfloat16 [2048, 32], replicated, may hold values from -0.125 to 0.125
- gate_w: bfloat16 [2048, 2048], P(None, 'tp'), may hold values from -0.125 to 0.125
- query_norm_gain: float32 [512], replicated, may hold values from 0.1 to 1.9
- latent_norm_gain: float32 [256], replicated, may hold values from 0.1 to 1.9
- query_plain_weight: bfloat16 [512, 2048], P(None, 'tp'), may hold values from -0.25 to 0.25
- query_rotary_weight: bfloat16 [512, 1024], P(None, 'tp'), may hold values from -0.25 to 0.25
- key_expand_weight: bfloat16 [256, 2048], P(None, 'tp'), may hold values from -0.375 to 0.375
- value_expand_weight: bfloat16 [256, 2048], P(None, 'tp'), may hold values from -0.375 to 0.375
- out_w: bfloat16 [2048, 2048], P('tp'), may hold values from -0.5 to 0.5
- norm_gain: float32 [2048], replicated, may hold values from 0.1 to 1.9
- norm_bias: float32 [2048], replicated, may hold values from -3 to 3
Outputs:
- mixed_out: bfloat16 [10240, 2048], P(('sp', 'tp'))
Inputs may be any that keep to these rules, and one draw needn't show every extreme that they name: `latents`: latent rows are noise plus three slow waves along the whole sequence. Most context rows have their own scales of 1 to 3; a few rows may be far larger.
All inputs are finite; a program needn't handle non-finite values.
Results may differ from a plain program's by a relative error of at most 0.024.
The roundings to bfloat16 on the way count: a program that leaves them out, or rounds other values in their place, can miss the bound.
Values may be sent and summed in bfloat16 or wider, within the bound.
A program may use at most 128 MiB of HBM per device.

v0:
```python
import jax
import jax.numpy as jnp
from jax import lax
from jax.sharding import Mesh
from jax.sharding import PartitionSpec as P

PLAIN_HEAD_SIZE = 64
ROTARY_SIZE = 32
VALUE_HEAD_SIZE = 64
GRID_W = 64
TP = ("tp_0", "tp_1")
SP = ("sp_0", "sp_1")
SP_TP = ("sp_0", "sp_1", "tp_0", "tp_1")


rope_base = 10000.0
norm_floor = 1e-06
residual_weight = 2.0**0.5
score_floor = -1e30


def one_axis_at_a_time(value, axes):
    for axis in axes:
        value = lax.psum(value, axis)
    return value


def in_one_piece(arrays, axis, dim, along):
    ends, at = ([], 0)
    for a in arrays[:-1]:
        at += a.shape[along]
        ends.append(at)
    both = jnp.concatenate(arrays, axis=along)
    return tuple(jnp.split(lax.all_gather(both, axis, axis=dim, tiled=True), ends, axis=along))


def in_order(pieces, dim):
    pieces = jnp.moveaxis(pieces, 0, dim)
    lengths = pieces.shape
    return pieces.reshape(*lengths[:dim], lengths[dim] * lengths[dim + 1], *lengths[dim + 2 :])


def all_blocks(value, axes, turns):
    pieces = value
    for k in turns:
        pieces = lax.all_gather(pieces, axes[k])
    done = turns[::-1]
    back = [done.index(k) for k in range(len(axes))]
    pieces = pieces.transpose(*back, *range(len(axes), pieces.ndim))
    return pieces.reshape(-1, *value.shape)


def whole_of(value, axes, turns, dim):
    return in_order(all_blocks(value, axes, turns), dim)


def rms_scale(values, gain):
    return values * lax.rsqrt(jnp.mean(values * values, axis=-1, keepdims=True) + norm_floor) * gain


def rotate(values, positions):
    pair_count = ROTARY_SIZE // 4
    inverse = rope_base ** (-jnp.arange(pair_count, dtype=jnp.float32) / pair_count)
    grid_row = (positions // GRID_W).astype(jnp.float32)
    grid_col = (positions % GRID_W).astype(jnp.float32)
    angles = jnp.stack([grid_row[:, None] * inverse, grid_col[:, None] * inverse], axis=1)
    cosine = jnp.cos(angles)[:, None, :, None, :]
    sine_part = jnp.sin(angles)[:, None, :, None, :]
    shaped = values.reshape(values.shape[0], -1, 2, 2, pair_count)
    first_part = shaped[:, :, :, 0:1, :]
    second = shaped[:, :, :, 1:2, :]
    turned = jnp.concatenate(
        [first_part * cosine - second * sine_part, second * cosine + first_part * sine_part], axis=3
    )
    return turned.reshape(values.shape)


def project(rows, weight):
    return jnp.dot(rows, weight, preferred_element_type=jnp.float32)


def per_device(
    latents,
    context,
    cond_vec,
    ctx_vec,
    shift_w,
    scale_w,
    modgate_w,
    query_down_weight,
    latent_down_weight,
    rot_down,
    gate_w,
    query_norm_gain,
    latent_norm_gain,
    query_plain_weight,
    query_rotary_weight,
    key_expand_weight,
    value_expand_weight,
    out_w,
    norm_gain,
    norm_bias,
):
    width_tp = lax.axis_size(TP)
    block_rows = latents.shape[0]
    seq_rows = block_rows * width_tp
    slab_rows = shift_w.shape[0]
    sp_index = lax.axis_index(SP)
    cond_rows = jnp.stack([jax.nn.silu(cond_vec), jax.nn.silu(ctx_vec)]).astype(jnp.bfloat16)
    cond_here = lax.dynamic_slice_in_dim(cond_rows, sp_index * slab_rows, slab_rows, 1)
    shift_part = project(cond_here, shift_w)
    scale_part = project(cond_here, scale_w)
    gate_part = project(cond_here, modgate_w)
    shift_rows, scale_rows, gate_rows = (
        one_axis_at_a_time(shift_part, SP),
        one_axis_at_a_time(scale_part, SP),
        one_axis_at_a_time(gate_part, SP),
    )
    shift_vec, scale_vec, gate_vec = in_one_piece((shift_rows, scale_rows, gate_rows), TP, 1, 0)
    latent_in = (latents.astype(jnp.float32) * (1.0 + scale_vec[0]) + shift_vec[0]).astype(
        jnp.bfloat16
    )
    context_in = (context.astype(jnp.float32) * (1.0 + scale_vec[1]) + shift_vec[1]).astype(
        jnp.bfloat16
    )
    heads_here = gate_w.shape[1] // VALUE_HEAD_SIZE
    rows_part = whole_of(latent_in, ("tp_0", "tp_1"), (0, 1), 0)
    positions = sp_index * seq_rows + jnp.arange(rows_part.shape[0], dtype=jnp.int32)
    q_codes = rms_scale(project(rows_part, query_down_weight), query_norm_gain).astype(jnp.bfloat16)
    kv_codes = rms_scale(project(rows_part, latent_down_weight), latent_norm_gain).astype(
        jnp.bfloat16
    )
    key_rot = rotate(project(rows_part, rot_down), positions).astype(jnp.bfloat16)
    gate_act = project(rows_part, gate_w).astype(jnp.bfloat16)
    project_q_cont = project(q_codes, query_plain_weight).astype(jnp.bfloat16)
    project_q_rot = rotate(project(q_codes, query_rotary_weight), positions).astype(jnp.bfloat16)
    joined = jnp.concatenate([project_q_cont, project_q_rot, gate_act, kv_codes, key_rot], axis=1)
    edge_one = query_plain_weight.shape[1]
    edge_two = edge_one + query_rotary_weight.shape[1]
    edge_three = edge_two + gate_w.shape[1]
    edge_four = edge_three + latent_down_weight.shape[1]
    q_cont = joined[:, :edge_one].reshape(seq_rows, heads_here, PLAIN_HEAD_SIZE)
    q_rot = joined[:, edge_one:edge_two].reshape(seq_rows, heads_here, ROTARY_SIZE)
    gate_act = joined[:, edge_two:edge_three]
    kv_codes = joined[:, edge_three:edge_four]
    key_rot = joined[:, edge_four:]
    ctx_codes = rms_scale(project(context_in, latent_down_weight), latent_norm_gain).astype(
        jnp.bfloat16
    )
    ctx_rot = project(context_in, rot_down).astype(jnp.bfloat16)
    score_scale = (PLAIN_HEAD_SIZE + ROTARY_SIZE) ** (-0.5)

    def expand(codes):
        return (
            project(codes, key_expand_weight).astype(jnp.bfloat16),
            project(codes, value_expand_weight).astype(jnp.bfloat16),
        )

    def attend(running, key_block, value_block, rotary):
        row_top, row_total, weighted = running
        key_count = key_block.shape[0]
        scores = jnp.einsum(
            "qhd,khd->hqk",
            q_cont,
            key_block.reshape(key_count, heads_here, PLAIN_HEAD_SIZE),
            preferred_element_type=jnp.float32,
        )
        scores = (
            scores + jnp.einsum("qhd,kd->hqk", q_rot, rotary, preferred_element_type=jnp.float32)
        ) * score_scale
        new_top = jnp.maximum(row_top, jnp.max(scores, axis=-1))
        weights = jnp.exp(scores - new_top[:, :, None])
        factor = jnp.exp(row_top - new_top)
        row_total = row_total * factor + jnp.sum(weights, axis=-1)
        weighted = weighted * factor[:, :, None] + jnp.einsum(
            "hqk,khd->hqd",
            weights.astype(jnp.bfloat16),
            value_block.reshape(key_count, heads_here, VALUE_HEAD_SIZE),
            preferred_element_type=jnp.float32,
        )
        return (new_top, row_total, weighted)

    start_state = (
        jnp.full((heads_here, seq_rows), score_floor, jnp.float32),
        jnp.zeros((heads_here, seq_rows), jnp.float32),
        jnp.zeros((heads_here, seq_rows, VALUE_HEAD_SIZE), jnp.float32),
    )
    ctx_all_codes, ctx_all_rot = in_one_piece((ctx_codes, ctx_rot), SP, 0, 1)
    ctx_keys, ctx_values = expand(ctx_all_codes)
    running = attend(start_state, ctx_keys, ctx_values, ctx_all_rot)
    pieces = in_one_piece((kv_codes, key_rot), SP, 0, 1)
    total_rows = pieces[0].shape[0]
    unit_count = total_rows // seq_rows
    grouped = max(
        [1]
        + [
            divisor
            for divisor in range(1, unit_count + 1)
            if unit_count % divisor == 0 and divisor * seq_rows <= 1024
        ]
    )
    blocked = tuple(
        (
            member.reshape(unit_count // grouped, grouped * seq_rows, member.shape[1])
            for member in pieces
        )
    )

    def one_block(carried, members):
        key_block, value_block = expand(members[0])
        return (attend(carried, key_block, value_block, members[1]), None)

    result, unused = lax.scan(one_block, running, blocked)
    running = result
    row_top, row_total, weighted = running
    attended = jnp.transpose(weighted / row_total[:, :, None], (1, 0, 2)).reshape(
        seq_rows, heads_here * VALUE_HEAD_SIZE
    )
    gated = (attended * jax.nn.silu(gate_act.astype(jnp.float32))).astype(jnp.bfloat16)
    own_rows = lax.all_to_all(gated, TP, split_axis=0, concat_axis=1, tiled=True)
    branch = project(own_rows, lax.all_gather(out_w, TP, axis=0, tiled=True))
    blended = residual_weight * latents.astype(jnp.float32) + gate_vec[0] * branch
    row_mean = jnp.mean(blended, axis=-1, keepdims=True)
    centred = blended - row_mean
    row_var = jnp.mean(centred * centred, axis=-1, keepdims=True)
    return (centred * lax.rsqrt(row_var + norm_floor) * norm_gain + norm_bias).astype(jnp.bfloat16)


def solution(mesh):
    split = Mesh(mesh.devices.reshape(8, 4, 4, 2), ("sp_0", "sp_1", "tp_0", "tp_1"))
    return jax.shard_map(
        per_device,
        mesh=split,
        in_specs=(
            P(SP_TP, None),
            P(SP, None),
            P(),
            P(),
            P(SP, TP),
            P(SP, TP),
            P(SP, TP),
            P(),
            P(),
            P(),
            P(None, TP),
            P(),
            P(),
            P(None, TP),
            P(None, TP),
            P(None, TP),
            P(None, TP),
            P(TP, None),
            P(),
            P(),
        ),
        out_specs=P(SP_TP, None),
        check_vma=False,
    )
```

profile of v0, /device:TPU:1, one launch (start us, length us, event | category | flops | bytes accessed | tf_op | source)
XLA Modules:
  0.0 334.3 jit_solution(8083279197834987134)
XLA Ops:
  11.0 17.5 %all-reduce = (f32[2,256]{1,0:T(2,128)S(1)}, f32[2,256]{1,0:T(2,128)S(1)}, f32[2,256]{1,0:T(2,128)S(1)}) all-reduce(f32[2,256]{1,0:T(2,128)S(1)} %fusion.51, f32[2,256]{1,0:T(2,128)S(1)} %fusion.47, f32[2,256]{1,0:T(2,128)S(1)} %fusion.49), channel_id=1, replica_groups=mesh['sp_0'=8,'sp_1'=4,'tp_0'=4,'tp_1'=2] {'sp_0'}, use_global_device_ids=true, to_apply=%region_4.5 | all-reduce | flops 1536 | bytes 12288 | tf_op jit(solution)/shard_map/psum | solution.py:24
  28.5 8.8 %all-reduce.1 = (f32[2,256]{1,0:T(2,128)S(1)}, f32[2,256]{1,0:T(2,128)S(1)}, f32[2,256]{1,0:T(2,128)S(1)}) all-reduce(f32[2,256]{1,0:T(2,128)S(1)} %get-tuple-element.120, f32[2,256]{1,0:T(2,128)S(1)} %get-tuple-element.121, f32[2,256]{1,0:T(2,128)S(1)} %get-tuple-element.122), channel_id=1, replica_groups=mesh['sp_0'=8,'sp_1'=4,'tp_0'=4,'tp_1'=2] {'sp_1'}, use_global_device_ids=true, to_apply=%region_5.6 | all-reduce | flops 1536 | bytes 12288 | tf_op jit(solution)/shard_map/psum | solution.py:24
  37.3 19.2 %all_gather.24 = f32[6,2048]{1,0:T(8,128)S(1)} all-gather(f32[6,256]{1,0:T(8,128)S(1)} %pad_maximum_fusion.5), channel_id=1, replica_groups=mesh['sp_0'=8,'sp_1'=4,'tp_0'=4,'tp_1'=2] {'tp_0','tp_1'}, dimensions={1}, use_global_device_ids=true | all-gather | bytes 55296 | tf_op jit(solution)/shard_map/all_gather | solution.py:34
  57.6 11.5 %all-gather = bf16[160,2048]{1,0:T(8,128)(2,1)} all-gather(bf16[40,2048]{1,0:T(8,128)(2,1)S(1)} %fusion.32), channel_id=2, replica_groups=mesh['sp_0'=8,'sp_1'=4,'tp_0'=4,'tp_1'=2] {'tp_0'}, dimensions={0}, use_global_device_ids=true | all-gather | bytes 819200 | tf_op jit(solution)/shard_map/all_gather | solution.py:46
  69.3 13.3 %all-gather.9.cloned.1.call-done = bf16[8,40,2048]{2,1,0:T(8,128)(2,1)} async-done(((bf16[4,40,2048]{2,1,0:T(8,128)(2,1)}), bf16[8,40,2048]{2,1,0:T(8,128)(2,1)}) %all-gather.9.cloned.1.call-update) | async-done | bytes 1310736 | tf_op jit(solution)/shard_map/all_gather | solution.py:46
  82.5 1.5 copy.48
  87.3 1.7 multiply_reduce_fusion.3
  90.2 41.4 %all_gather.29 = bf16[1024,288]{1,0:T(8,128)(2,1)S(1)} all-gather(bf16[32,288]{1,0:T(8,128)(2,1)S(1)} %pad_maximum_fusion.1), channel_id=1, replica_groups=mesh['sp_0'=8,'sp_1'=4,'tp_0'=4,'tp_1'=2] {'sp_0','sp_1'}, dimensions={0}, use_global_device_ids=true | all-gather | bytes 608256 | tf_op jit(solution)/shard_map/all_gather | solution.py:34
  140.1 38.8 %all-gather.11.cloned.1.call-done = bf16[32,320,288]{1,2,0:T(8,128)(2,1)} async-done(((bf16[1,320,288]{1,2,0:T(8,128)(2,1)}), bf16[32,320,288]{1,2,0:T(8,128)(2,1)}) %all-gather.11.cloned.1.call-update) | async-done | bytes 5898256 | tf_op jit(solution)/shard_map/all_gather | solution.py:34
  178.9 8.5 %copy.54 = bf16[32,320,288]{1,0,2:T(8,128)(2,1)} copy(bf16[32,320,288]{1,2,0:T(8,128)(2,1)} %all-gather.11.cloned.1.call-done) | data formatting | bytes 11796480 | tf_op jit(solution)/shard_map/all_gather | solution.py:34
  187.3 13.0 %reshape.344 = bf16[10240,288]{0,1:T(8,128)(2,1)} reshape(bf16[32,320,288]{1,0,2:T(8,128)(2,1)} %copy.54) | data formatting | bytes 11796480
  200.3 5.4 %split.21 = bf16[10240,256]{0,1:T(8,128)(2,1)} slice(bf16[10240,288]{0,1:T(8,128)(2,1)} %reshape.344), slice={[0:10240], [0:256]} | slice | bytes 10485760 | tf_op jit(solution)/shard_map/split | solution.py:34
  205.8 8.0 %copy.63 = bf16[10240,256]{1,0:T(8,128)(2,1)} copy(bf16[10240,256]{0,1:T(8,128)(2,1)} %split.21) | data formatting | bytes 10485760 | tf_op jit(solution)/shard_map/while | solution.py:213
  213.8 94.4 %while.14 = (s32[]{:T(128)}, f32[4,320]{1,0:T(4,128)S(1)}, f32[4,320]{1,0:T(4,128)S(1)}, f32[4,320,64]{1,2,0:T(8,128)S(1)}, bf16[16,640,256]{2,1,0:T(8,128)(2,1)...) while((s32[]{:T(128)}, f32[4,320]{1,0:T(4,128)S(1)}, ...), condition=%wide.region_14.15_spmd, body=%wide.region_11.14_spmd.sunk | while | flops 436144640 | bytes 19653744 | solution.py:213
  217.6 1.3 convolution_convert_fusion.10
  223.5 1.3 convolution_convert_fusion.10
  229.4 1.3 convolution_convert_fusion.10
  231.6 1.3 convolution_convert_fusion.9
  235.3 1.3 convolution_convert_fusion.10
  241.2 1.3 convolution_convert_fusion.10
  247.1 1.3 convolution_convert_fusion.10
  249.3 1.3 convolution_convert_fusion.9
  253.0 1.3 convolution_convert_fusion.10
  258.9 1.3 convolution_convert_fusion.10
  264.8 1.3 convolution_convert_fusion.10
  267.0 1.3 convolution_convert_fusion.9
  270.7 1.3 convolution_convert_fusion.10
  282.5 1.3 convolution_convert_fusion.10
  300.1 1.3 convolution_convert_fusion.10
  308.4 2.2 multiply_convert_fusion.1
  310.6 10.8 %all_to_all.19 = bf16[8,40,256]{2,1,0:T(8,128)(2,1)S(1)} all-to-all(bf16[8,40,256]{2,1,0:T(8,128)(2,1)S(1)} %bitcast.145), channel_id=1, replica_groups=mesh['sp_0'=8,'sp_1'=4,'tp_0'=4,'tp_1'=2] {'tp_0','tp_1'}, dimensions={0} | all-to-all | bytes 327680 | tf_op jit(solution)/shard_map/all_to_all | solution.py:220
  321.5 5.2 %fusion.57 = (f32[40]{0:T(128)S(1)}, f32[40,2048]{1,0:T(8,128)S(1)}) fusion(bf16[40,2048]{1,0:T(8,128)(2,1)S(1)} %bitcast.136, bf16[2048,2048]{1,0:T(8,128)(2,1)} %all-gather.7.cloned.1.call-done, f32[2048]{0:T(1024)S(1)} %bitcast.147, bf16[40,2048]{1,0:T(8,128)(2,1)S(1)} %copy-done.9), kind=kOutput, calls=%fused_computation.112 | convolution fusion | flops 335953888 | bytes 9052320 | tf_op jit(solution)/shard_map/dot_general | solution.py:79
  (224 shorter events, 94.0 us)
Async XLA Ops:
  6.5 127.4 %copy-start = (bf16[2048,512]{1,0:T(8,128)(2,1)S(1)}, bf16[2048,512]{1,0:T(8,128)(2,1)}, u32[]{:S(2)}) copy-start(bf16[2048,512]{1,0:T(8,128)(2,1)} %param.29) | copy-start | bytes 6291460
  6.5 77.5 %copy-start.8 = (bf16[2048,256]{1,0:T(8,128)(2,1)S(1)}, bf16[2048,256]{1,0:T(8,128)(2,1)}, u32[]{:S(2)}) copy-start(bf16[2048,256]{1,0:T(8,128)(2,1)} %param.30) | copy-start | bytes 3145732
  6.5 76.0 %all-gather.9.cloned.1.call-start = ((), (), s32[]{:S(2)}) async-start(), calls=%async_computation.2 | async-start | bytes 1966080 | tf_op jit(solution)/shard_map/all_gather | solution.py:46
  69.1 109.7 %all-gather.11.cloned.1.call-start = ((), (), s32[]{:S(2)}) async-start(), calls=%async_computation.3 | async-start | bytes 7299072 | tf_op jit(solution)/shard_map/all_gather | solution.py:34
  82.5 2.2 copy-start.17
  84.0 1.2 copy-start.6
  84.1 1.4 copy-start.16
  84.7 2.6 copy-start.11
  85.2 46.3 %copy-start.2 = (bf16[256,256]{1,0:T(8,128)(2,1)S(1)}, bf16[256,256]{1,0:T(8,128)(2,1)}, u32[]{:S(2)}) copy-start(bf16[256,256]{1,0:T(8,128)(2,1)} %param.37) | copy-start | bytes 393220
  85.3 47.3 %copy-start.3 = (bf16[256,256]{1,0:T(8,128)(2,1)S(1)}, bf16[256,256]{1,0:T(8,128)(2,1)}, u32[]{:S(2)}) copy-start(bf16[256,256]{1,0:T(8,128)(2,1)} %param.38) | copy-start | bytes 393220
  86.5 234.9 %all-gather.7.cloned.1.call-start = ((), (), s32[]{:S(2)}) async-start(), calls=%async_computation.1 | async-start | bytes 9437184 | tf_op jit(solution)/shard_map/all_gather | solution.py:221
  87.3 46.7 %copy-start.7 = (bf16[4,2,40,2048]{3,2,1,0:T(8,128)(2,1)S(1)}, bf16[4,2,40,2048]{3,2,1,0:T(8,128)(2,1)}, u32[]{:S(2)}) copy-start(bf16[4,2,40,2048]{3,2,1,0:T(8,128)(2,1)} %copy-done.6) | copy-start | bytes 3932164
  132.7 2.3 copy-start.12
  132.7 2.3 copy-start.15
  133.9 1.3 copy-start.10
  134.9 1.0 copy-start.4
  137.9 1.2 copy-start.5
  205.8 8.0 %slice-start = ((bf16[10240,288]{0,1:T(8,128)(2,1)}), bf16[10240,32]{0,1:T(8,128)(2,1)S(1)}, s32[]{:S(2)}) async-start(bf16[10240,288]{0,1:T(8,128)(2,1)} %reshape.344), calls=%async_computation.4 | async-start | bytes 1310720 | tf_op jit(solution)/shard_map/split | solution.py:34
  308.4 13.1 %copy-start.9 = (bf16[40,2048]{1,0:T(8,128)(2,1)S(1)}, bf16[40,2048]{1,0:T(8,128)(2,1)}, u32[]{:S(2)}) copy-start(bf16[40,2048]{1,0:T(8,128)(2,1)} %param.22) | copy-start | bytes 491524
  321.5 5.5 %copy-start.13 = (f32[2048]{0:T(1024)S(1)}, f32[2048]{0:T(1024)}, u32[]{:S(2)}) copy-start(f32[2048]{0:T(1024)} %param.41) | copy-start | bytes 24580
  321.5 5.5 %copy-start.14 = (f32[2048]{0:T(1024)S(1)}, f32[2048]{0:T(1024)}, u32[]{:S(2)}) copy-start(f32[2048]{0:T(1024)} %param.40) | copy-start | bytes 24580
  321.5 6.3 %copy-start.1 = (bf16[2048,512]{1,0:T(8,128)(2,1)S(1)}, bf16[2048,512]{1,0:T(8,128)(2,1)}, u32[]{:S(2)}) copy-start(bf16[2048,512]{1,0:T(8,128)(2,1)} %param.29) | copy-start | bytes 6291460
Sparse Core Ops, SparseCore 0:
  69.2 13.2 all-gather.8
  86.6 92.1 all-gather.10
  180.7 50.2 all-gather.6
where the time goes:
time: 337 us; the launch traced here: 334 us
  blocking collectives  109 us (32%)
  matrix products  98.4 us (29%)
  waiting for transfers between devices  52.8 us (16%)
  local copies, waits for them, and re-layouts  38 us (11%)
  other arithmetic  21.4 us (6%)
  between operations  13.6 us (4%)
    all_gather x2, blocking collectives, in_one_piece(): lax.all_gather(both, axis, axis=dim, tiled=True)  60.6 us
    dot_general x46, matrix products, project(): return jnp.dot(rows, weight, preferred_element_type=jnp.float32)  58.9 us
    all_gather x1, waiting for transfers between devices, in_one_piece(): lax.all_gather(both, axis, axis=dim, tiled=True)  38.8 us
    psum x2, blocking collectives, one_axis_at_a_time(): value = lax.psum(value, axis)  26.3 us
    reduce_sum x17, other arithmetic, attend(): row_total = row_total * factor + jnp.sum(weights, axis=-1)  16.7 us
    dot_general x17, matrix products, attend(): jnp.einsum('hqk,khd->hqd', weights.astype(jnp.bfloat16), value_block.resh...  14.7 us
    unnamed x38, local copies, waits for them, and re-layouts  14 us
    dot_general x17, matrix products, attend(): jnp.einsum('qhd,kd->hqk', q_rot, rotary, preferred_element_type=jnp.float32)  13.9 us
  transfers between devices with their start and end apart: 3, of which 2 were waited for; matrix products, arithmetic and copies ran while one was open for 43% of the time, Pallas kernels for 0%

commit v1 on v0

v1 whole, which is shorter than its diff:
```python
import math

import jax
import jax.numpy as jnp
import numpy as np
from jax import lax
from jax.experimental import pallas as pl
from jax.experimental.pallas import tpu as pltpu
from jax.sharding import PartitionSpec as P

F32, BF16 = jnp.float32, jnp.bfloat16
NZ, NY, NX, NC = 8, 4, 4, 2
NTP = NX * NC
ROWS = 40
SLAB = 320
HALF = 160
CTXH = 16
PIECE = HALF + CTXH
MSG = PIECE + 32
CUT = 112
UNIT = 2 * NY * PIECE
WIDTH = 2048
COL = 256
EPS = 1e-06
SQRT2 = 2.0**0.5
SCORE = math.log2(math.e) / math.sqrt(96.0)


def rope_tables():
    inverse = (10000.0 ** (-np.arange(8, dtype=np.float64) / 8)).astype(np.float32)
    lane = np.arange(128)
    axis, member, pair = (lane // 16) % 2, (lane // 8) % 2, lane % 8
    sign = np.where(member == 0, -1.0, 1.0)

    def rows_of(numbers, which):
        angle = (numbers[:, None].astype(np.float32) * inverse[pair][None, :]).astype(np.float64)
        keep = axis[None, :] == which
        return np.where(keep, np.cos(angle), 0.0), np.where(keep, np.sin(angle) * sign, 0.0)

    cos_row, sin_row = rows_of(np.arange(160), 0)
    cos_col, sin_col = rows_of(np.arange(64), 1)
    by_slab = np.zeros((32, 16, 128), np.float32)
    by_slab[:, 0:5] = cos_row.reshape(32, 5, 128)
    by_slab[:, 8:13] = sin_row.reshape(32, 5, 128)
    return by_slab, np.concatenate([cos_col, sin_col], 0).astype(np.float32)


def dot(a, b):
    return jnp.dot(a, b, preferred_element_type=F32)


def silu(v):
    return v / (1.0 + jnp.exp(-v))


def rms(v, gain):
    return v * lax.rsqrt(jnp.mean(v * v, axis=-1, keepdims=True) + EPS) * gain


def swap_members(v):
    lane = lax.broadcasted_iota(jnp.int32, v.shape, 1)
    return jnp.where(lane % 16 < 8, pltpu.roll(v, 120, 1), pltpu.roll(v, 8, 1))


def body(
    lat_h, ctx_h, cond_h, ctxv_h, shw_h, scw_h, mgw_h, qd_h, ld_h, rd_h, gw_h, qg_h, kg_h, qp_h, qr_h, ke_h, ve_h,
    ow_h, ng_h, nb_h, rrow_h, rcol_h, out,
    gath, ctx_v, cond_v, ctxv_v, w3, qd, ld, rd, gw, qg, kg, qp, qr, ke, ve, ow, ng, nb, rrow, rcol,
    ybuf, zbuf, mod, xin, xc, tabc, tabs, kv, ket, q2, kt2, acc, top, total, sgate, gsrc, gdst,
    lsem, ysend, yrecv, zsend, zrecv, tsend, trecv, lx_send, lx_recv, kz_send, kz_recv, ky_send, ky_recv,
    kd_send, kd_recv, ox_send, ox_recv, a_send, a_recv,
):
    sp, tp = lax.axis_index("sp"), lax.axis_index("tp")
    z, y, x, c = sp // NY, sp % NY, tp // NC, tp % NC

    def at_z(d):
        return {"sp": ((z + d) % NZ) * NY + y, "tp": tp}

    def at_y(d):
        return {"sp": z * NY + (y + d) % NY, "tp": tp}

    def slot_x(d):
        return ((x + d) % NX) * NC + c

    def at_x(d):
        return {"sp": sp, "tp": slot_x(d)}

    partner_slot = x * NC + (1 - c)
    partner = {"sp": sp, "tp": partner_slot}

    def at_tp(d):
        return {"sp": sp, "tp": (tp + d) % NTP}

    def push(src, dst, send, recv, to):
        pltpu.make_async_remote_copy(
            src_ref=src, dst_ref=dst, send_sem=send, recv_sem=recv, device_id=to, device_id_type=pl.DeviceIdType.MESH
        ).start()

    def take(ref, sem):
        pltpu.make_async_copy(ref, ref, sem).wait()

    local = [
        (cond_h, cond_v), (ctxv_h, ctxv_v), (shw_h, w3.at[0]), (scw_h, w3.at[1]), (mgw_h, w3.at[2]),
        (lat_h, gath.at[tp]), (ctx_h, ctx_v), (ld_h, ld), (rd_h, rd), (rrow_h.at[sp], rrow), (rcol_h, rcol),
        (kg_h, kg), (qd_h, qd), (qg_h, qg), (qp_h, qp), (qr_h, qr), (gw_h, gw), (ke_h, ke), (ve_h, ve),
        (ow_h, ow.at[tp]), (ng_h, ng), (nb_h, nb),
    ]
    for k, (src, dst) in enumerate(local):
        pltpu.make_async_copy(src, dst, lsem.at[k]).start()

    def have(*which):
        for k in which:
            take(local[k][1], lsem.at[k])

    barrier = pltpu.get_barrier_semaphore()
    peers = [at_y(d) for d in range(1, NY)] + [at_z(d) for d in range(1, NZ)] + [at_tp(d) for d in range(1, NTP)]
    for peer in peers:
        pl.semaphore_signal(barrier, inc=1, device_id=peer, device_id_type=pl.DeviceIdType.MESH)

    have(0, 1, 2, 3, 4)
    pick = pl.ds(sp // 2, 1)
    lane = lax.broadcasted_iota(jnp.int32, (8, 128), 1)
    line = lax.broadcasted_iota(jnp.int32, (8, 128), 0)
    mine = lane // 64 == sp % 2
    cond_row = jnp.broadcast_to(silu(cond_v[pick, :]), (8, 128))
    ctxv_row = jnp.broadcast_to(silu(ctxv_v[pick, :]), (8, 128))
    part = jnp.zeros((8, COL), F32)
    for k in range(3):
        rows = jnp.where(line == 2 * k, cond_row, jnp.where(line == 2 * k + 1, ctxv_row, 0.0))
        rows = jnp.where(mine, rows, 0.0).astype(BF16)
        part = part + dot(rows, jnp.concatenate([w3[k], w3[k]], axis=0))
    ybuf[y] = part
    pl.semaphore_wait(barrier, len(peers))

    for d in range(1, NY):
        push(ybuf.at[y], ybuf.at[y], ysend.at[d - 1], yrecv.at[d - 1], at_y(d))
    have(5)
    own = gath.at[tp]
    push(own, own, lx_send.at[0], lx_recv.at[0], at_x(1))
    push(own, own, lx_send.at[1], lx_recv.at[1], at_x(-1))
    push(own, own, lx_send.at[2], lx_recv.at[2], partner)
    for d in range(1, NY):
        take(ybuf.at[(y - d) % NY], yrecv.at[d - 1])
    zbuf[z] = (ybuf[0] + ybuf[1]) + (ybuf[2] + ybuf[3])
    for d in range(1, NZ):
        push(zbuf.at[z], zbuf.at[z], zsend.at[d - 1], zrecv.at[d - 1], at_z(d))

    left, right, across = slot_x(-1), slot_x(1), slot_x(2)
    first, second = pl.ds(0, WIDTH // 2), pl.ds(WIDTH // 2, WIDTH // 2)
    take(gath.at[left], lx_recv.at[0])
    push(gath.at[left, :, first], gath.at[left, :, first], lx_send.at[3], lx_recv.at[3], at_x(1))
    push(gath.at[left], gath.at[left], lx_send.at[4], lx_recv.at[4], partner)
    take(gath.at[right], lx_recv.at[1])
    push(gath.at[right, :, second], gath.at[right, :, second], lx_send.at[5], lx_recv.at[5], at_x(-1))
    push(gath.at[right], gath.at[right], lx_send.at[6], lx_recv.at[6], partner)

    for d in range(1, NZ):
        take(zbuf.at[(z - d) % NZ], zrecv.at[d - 1])
    whole = zbuf[0]
    for k in range(1, NZ):
        whole = whole + zbuf[k]
    mod[tp] = whole
    for d in range(1, NTP):
        push(mod.at[tp], mod.at[tp], tsend.at[d - 1], trecv.at[d - 1], at_tp(d))

    have(9, 10, 17)
    for k in range(5):
        rows = pl.ds(64 * k, 64)
        tabc[rows, :] = rrow[k : k + 1, :] + rcol[0:64, :]
        tabs[rows, :] = rrow[8 + k : 9 + k, :] + rcol[64:128, :]
    ket[...] = ke[...].astype(F32).T.astype(BF16)
    top[...] = jnp.full(top.shape, -1e30, F32)
    total[...] = jnp.zeros(total.shape, F32)
    acc[...] = jnp.zeros(acc.shape, F32)

    take(gath.at[across, :, first], lx_recv.at[3])
    take(gath.at[across, :, second], lx_recv.at[5])
    push(gath.at[across], gath.at[across], lx_send.at[7], lx_recv.at[7], partner)

    for d in range(1, NTP):
        take(mod.at[(tp - d) % NTP], trecv.at[d - 1])
    have(19)
    owned = ow.at[tp]
    push(owned, owned, ox_send.at[0], ox_recv.at[0], at_x(1))
    push(owned, owned, ox_send.at[1], ox_recv.at[1], at_x(-1))
    push(owned, owned, ox_send.at[2], ox_recv.at[2], partner)

    def vector(row):
        return jnp.concatenate([mod[t, row : row + 1, :] for t in range(NTP)], axis=1)

    take(gath.at[partner_slot], lx_recv.at[2])
    for n, d in ((4, -1), (6, 1), (7, 2)):
        take(gath.at[((x + d) % NX) * NC + (1 - c)], lx_recv.at[n])
    shift, scale = vector(0), 1.0 + vector(2)
    for p in range(NTP // 2):
        pair = jnp.concatenate([gath[2 * p].astype(F32), gath[2 * p + 1].astype(F32)], axis=0)
        xin[2 * ROWS * p : 2 * ROWS * (p + 1), :] = (pair * scale + shift).astype(BF16)
    have(6)
    xc[...] = (ctx_v[...].astype(F32) * (1.0 + vector(3)) + vector(1)).astype(BF16)

    have(7, 8, 11)
    half = pl.ds(pl.multiple_of(HALF * c, HALF), HALF)
    mine_in = jnp.concatenate([xin[half, :], xc[pl.ds(pl.multiple_of(CTXH * c, CTXH), CTXH), :]], axis=0)
    slot = NY * c + y
    kv[z, slot, 0:PIECE, :] = rms(dot(mine_in, ld[...]), kg[...]).astype(BF16)
    flat = jnp.concatenate([dot(mine_in, rd[...]), jnp.zeros((PIECE, 96), F32)], axis=1)
    lat_part = flat[0:HALF]
    turned = lat_part * tabc[half, :] + swap_members(lat_part) * tabs[half, :]
    both = jnp.concatenate([turned, flat[HALF:], jnp.zeros((256 - PIECE, 128), F32)], axis=0)
    kv[z, slot, PIECE:MSG, :] = both.T[0:32, :].astype(BF16)

    def z_of(i):
        off = (i % 2) * ((i + 1) // 2) - (1 - i % 2) * (i // 2)
        return (z + off + NZ) % NZ

    low, high = pl.ds(0, CUT), pl.ds(CUT, MSG - CUT)

    def stage_z(i):
        here = kv.at[z_of(i), slot]

        def when(test, act):
            if isinstance(test, bool):
                if test:
                    act()
            else:
                pl.when(test)(act)

        def forward_whole():
            to = {"sp": ((z + NZ + 1 - 2 * (i % 2)) % NZ) * NY + y, "tp": tp}
            push(here, here, kz_send.at[i + 2], kz_recv.at[i + 2], to)

        def forward_low():
            push(here.at[low], here.at[low], kz_send.at[7], kz_recv.at[7], at_z(-1))

        def forward_high():
            push(here.at[high], here.at[high], kz_send.at[8], kz_recv.at[8], at_z(1))

        def take_whole():
            take(here, kz_recv.at[i])

        def take_parts():
            take(here.at[low], kz_recv.at[7])
            take(here.at[high], kz_recv.at[8])

        if isinstance(i, int) and i == 0:
            push(here, here, kz_send.at[1], kz_recv.at[1], at_z(-1))
            push(here, here, kz_send.at[2], kz_recv.at[2], at_z(1))
        else:
            when(i < 7, take_whole)
            when(i == 7, take_parts)
            when(i < 5, forward_whole)
            when(i == 5, forward_low)
            when(i == 6, forward_high)
        push(here, here, ky_send.at[i, 0], ky_recv.at[i, 0], at_y(1))
        push(here, here, ky_send.at[i, 1], ky_recv.at[i, 1], at_y(-1))

    def at_slot(i, d):
        return kv.at[z_of(i), NY * c + (y + d + NY) % NY]

    def stage_y(i):
        below, above = at_slot(i, -1), at_slot(i, 1)
        take(below, ky_recv.at[i, 0])
        push(below.at[low], below.at[low], ky_send.at[i, 2], ky_recv.at[i, 2], at_y(1))
        take(above, ky_recv.at[i, 1])
        push(above.at[high], above.at[high], ky_send.at[i, 3], ky_recv.at[i, 3], at_y(-1))

    def stage_d(i):
        far = at_slot(i, 2)
        take(far.at[low], ky_recv.at[i, 2])
        take(far.at[high], ky_recv.at[i, 3])
        four = kv.at[z_of(i), pl.ds(NY * c, NY)]
        push(four, four, kd_send.at[i], kd_recv.at[i], partner)

    stage_z(0)

    have(12, 13, 14, 15)
    q_codes = rms(dot(xin[...], qd[...]), qg[...]).astype(BF16)
    q_cont = dot(q_codes, qp[...]) * SCORE
    q_rot = dot(q_codes, qr[...])
    q_rot = (q_rot * tabc[...] + swap_members(q_rot) * tabs[...]) * SCORE
    q_lane = lax.broadcasted_iota(jnp.int32, (SLAB, 128), 1)
    for h in range(4):
        j, rows = h // 2, pl.ds(SLAB * (h % 2), SLAB)
        plain = q_cont[:, 128 * j : 128 * (j + 1)]
        q2[j, rows, 0:128] = jnp.where(q_lane // 64 == h % 2, plain, 0.0).astype(BF16)
        q2[j, rows, 128:256] = jnp.where(q_lane // 32 == h, q_rot, 0.0).astype(BF16)
    stage_z(1)
    stage_y(0)
    have(16)
    sgate[...] = silu(dot(xin[...], gw[...]).astype(BF16).astype(F32))
    stage_z(2)
    stage_y(1)
    stage_d(0)

    def one_unit(i, carry):
        @pl.when(i < 5)
        def _():
            stage_z(i + 3)

        @pl.when(i < 6)
        def _():
            stage_y(i + 2)

        @pl.when(i < 7)
        def _():
            stage_d(i + 1)

        @pl.when(i == 5)
        def _():
            take(ow.at[left], ox_recv.at[0])
            push(ow.at[left, pl.ds(0, 128)], ow.at[left, pl.ds(0, 128)], ox_send.at[3], ox_recv.at[3], at_x(1))
            push(ow.at[left], ow.at[left], ox_send.at[4], ox_recv.at[4], partner)
            take(ow.at[right], ox_recv.at[1])
            push(ow.at[right, pl.ds(128, 128)], ow.at[right, pl.ds(128, 128)], ox_send.at[5], ox_recv.at[5], at_x(-1))
            push(ow.at[right], ow.at[right], ox_send.at[6], ox_recv.at[6], partner)

        at = z_of(i)
        take(kv.at[at, pl.ds(NY * (1 - c), NY)], kd_recv.at[i])
        codes = jnp.concatenate([kv[at, p, 0:PIECE, :] for p in range(2 * NY)], axis=0)
        rot = jnp.concatenate([kv[at, p, PIECE:MSG, 0:PIECE] for p in range(2 * NY)], axis=1)
        keys = lax.dot_general(ket[...], codes, (((1,), (1,)), ((), ())), preferred_element_type=F32).astype(BF16)
        for j in range(2):
            kt2[j, 0:128, :] = keys[128 * j : 128 * (j + 1)]
            for h in range(4):
                kt2[j, 128 + 32 * h : 160 + 32 * h, :] = rot

        def scores(h):
            return dot(q2[h // 2, SLAB * (h % 2) : SLAB * (h % 2 + 1), :], kt2[h // 2])

        coming = scores(0)
        for h in range(4):
            s = coming
            if h < 3:
                coming = scores(h + 1)
            rows = pl.ds(SLAB * h, SLAB)
            old = top[rows, :]
            new = jnp.maximum(old, jnp.max(s, axis=1, keepdims=True))
            w = jnp.exp2(s - new)
            fade = jnp.exp2(old - new)
            top[rows, :] = new
            total[rows, :] = total[rows, :] * fade + jnp.sum(w, axis=1, keepdims=True)
            acc[rows, :] = acc[rows, :] * fade + dot(w.astype(BF16), codes)
        return carry

    lax.fori_loop(0, NZ, one_unit, 0)

    take(ow.at[across, pl.ds(0, 128)], ox_recv.at[3])
    take(ow.at[across, pl.ds(128, 128)], ox_recv.at[5])
    push(ow.at[across], ow.at[across], ox_send.at[7], ox_recv.at[7], partner)

    have(18)
    col = lax.broadcasted_iota(jnp.int32, (SLAB, COL), 1)
    attended = jnp.zeros((SLAB, COL), F32)
    for h in range(4):
        rows = pl.ds(SLAB * h, SLAB)
        inner = (acc[rows, :] / total[rows, :]).astype(BF16)
        attended = jnp.where(col // 64 == h, dot(inner, ve[...]), attended)
    gated = attended * sgate[...]
    for t in range(NTP):
        gsrc[t] = gated[ROWS * t : ROWS * (t + 1), :].astype(BF16)
    gdst[tp] = gsrc[tp]
    for d in range(1, NTP):
        push(gsrc.at[(tp + d) % NTP], gdst.at[tp], a_send.at[d - 1], a_recv.at[d - 1], at_tp(d))

    take(ow.at[partner_slot], ox_recv.at[2])
    for n, d in ((4, -1), (6, 1), (7, 2)):
        take(ow.at[((x + d) % NX) * NC + (1 - c)], ox_recv.at[n])
    for d in range(1, NTP):
        take(gdst.at[(tp - d) % NTP], a_recv.at[d - 1])
    have(20, 21)
    rows_in = jnp.concatenate([gdst[t] for t in range(NTP)], axis=1)
    branch = dot(rows_in, ow[...].reshape(WIDTH, WIDTH))
    blended = SQRT2 * gath[tp].astype(F32) + vector(4) * branch
    centred = blended - jnp.mean(blended, axis=-1, keepdims=True)
    spread = jnp.mean(centred * centred, axis=-1, keepdims=True)
    out[...] = (centred * lax.rsqrt(spread + EPS) * ng[...] + nb[...]).astype(BF16)

    for d in range(NY - 1):
        take(ybuf.at[y], ysend.at[d])
    for d in range(NZ - 1):
        take(zbuf.at[z], zsend.at[d])
    for d in range(NTP - 1):
        take(mod.at[tp], tsend.at[d])
        take(gdst.at[tp], a_send.at[d])
    for n in (0, 1, 2, 4, 6, 7):
        take(gath.at[tp], lx_send.at[n])
        take(ow.at[tp], ox_send.at[n])
    for n in (3, 5):
        take(gath.at[tp, :, first], lx_send.at[n])
        take(ow.at[tp, pl.ds(0, 128)], ox_send.at[n])
    here = kv.at[z, slot]
    for n in range(1, 7):
        take(here, kz_send.at[n])
    take(here.at[low], kz_send.at[7])
    take(here.at[high], kz_send.at[8])

    def drain(i, carry):
        take(here, ky_send.at[i, 0])
        take(here, ky_send.at[i, 1])
        take(here.at[low], ky_send.at[i, 2])
        take(here.at[high], ky_send.at[i, 3])
        take(kv.at[z, pl.ds(0, NY)], kd_send.at[i])
        return carry

    lax.fori_loop(0, NZ, drain, 0)


def per_device(
    latents, context, cond_vec, ctx_vec, shift_w, scale_w, modgate_w, query_down_weight, latent_down_weight, rot_down,
    gate_w, query_norm_gain, latent_norm_gain, query_plain_weight, query_rotary_weight, key_expand_weight,
    value_expand_weight, out_w, norm_gain, norm_bias,
):
    by_slab, by_col = rope_tables()
    args = (
        latents, context, cond_vec.reshape(16, 128), ctx_vec.reshape(16, 128), shift_w, scale_w, modgate_w,
        query_down_weight, latent_down_weight, rot_down, gate_w, query_norm_gain.reshape(1, 512),
        latent_norm_gain.reshape(1, COL), query_plain_weight, query_rotary_weight, key_expand_weight,
        value_expand_weight, out_w, norm_gain.reshape(1, WIDTH), norm_bias.reshape(1, WIDTH),
        jnp.asarray(by_slab), jnp.asarray(by_col),
    )
    vm = pltpu.VMEM
    dma = pltpu.SemaphoreType.DMA
    scratch = [
        vm((NTP, ROWS, WIDTH), BF16), vm((32, WIDTH), BF16), vm((16, 128), F32), vm((16, 128), F32),
        vm((3, 64, COL), BF16), vm((WIDTH, 512), BF16), vm((WIDTH, COL), BF16), vm((WIDTH, 32), BF16),
        vm((WIDTH, COL), BF16), vm((1, 512), F32), vm((1, COL), F32), vm((512, COL), BF16), vm((512, 128), BF16),
        vm((COL, COL), BF16), vm((COL, COL), BF16), vm((NTP, COL, WIDTH), BF16), vm((1, WIDTH), F32),
        vm((1, WIDTH), F32), vm((16, 128), F32), vm((128, 128), F32),
        vm((NY, 8, COL), F32), vm((NZ, 8, COL), F32), vm((NTP, 8, COL), F32), vm((SLAB, WIDTH), BF16),
        vm((32, WIDTH), BF16), vm((SLAB, 128), F32), vm((SLAB, 128), F32), vm((NZ, 2 * NY, MSG, COL), BF16),
        vm((COL, COL), BF16), vm((2, 2 * SLAB, COL), BF16), vm((2, COL, UNIT), BF16), vm((4 * SLAB, COL), F32),
        vm((4 * SLAB, 1), F32), vm((4 * SLAB, 1), F32), vm((SLAB, COL), F32), vm((NTP, ROWS, COL), BF16),
        vm((NTP, ROWS, COL), BF16),
        dma((22,)), dma((NY - 1,)), dma((NY - 1,)), dma((NZ - 1,)), dma((NZ - 1,)), dma((NTP - 1,)), dma((NTP - 1,)),
        dma((8,)), dma((8,)), dma((9,)), dma((9,)), dma((NZ, 4)), dma((NZ, 4)), dma((NZ,)), dma((NZ,)),
        dma((8,)), dma((8,)), dma((NTP - 1,)), dma((NTP - 1,)),
    ]
    return pl.pallas_call(
        body,
        out_shape=jax.ShapeDtypeStruct((ROWS, WIDTH), BF16),
        in_specs=[pl.BlockSpec(memory_space=pl.ANY)] * len(args),
        out_specs=pl.BlockSpec(memory_space=pltpu.VMEM),
        scratch_shapes=scratch,
        compiler_params=pltpu.CompilerParams(collective_id=0, has_side_effects=True, vmem_limit_bytes=62 * 1024 * 1024),
    )(*args)


def solution(mesh):
    tp, sp = P(None, "tp"), P("sp", "tp")
    return jax.shard_map(
        per_device,
        mesh=mesh,
        in_specs=(
            P(("sp", "tp"), None), P("sp", None), P(), P(), sp, sp, sp, P(), P(), P(), tp, P(), P(), tp, tp, tp, tp,
            P("tp", None), P(), P(),
        ),
        out_specs=P(("sp", "tp"), None),
        check_vma=False,
    )
```

time: 337 us -> 81.3 us (0.24)
  blocking collectives: 109 us -> 0 us
  matrix products: 98.4 us -> 0 us
  Pallas kernels: 0 us -> 77.7 us
  waiting for transfers between devices: 52.8 us -> 0 us
  local copies, waits for them, and re-layouts: 38 us -> 3.5 us
  other arithmetic: 21.4 us -> 0 us
  between operations: 13.6 us -> 0.01 us
    dot_general x97 -> x0, matrix products: 98.4 us -> none  [the longest x46 58.9 us: project(): return jnp.dot(rows, weight, preferred_element_type=jnp.float32)]
    pallas_call x0 -> x1, Pallas kernels: none -> 77.7 us  [per_device(): pl.pallas_call(body, out_shape=jax.ShapeDtypeStruct((ROWS, WIDTH), BF16),...]
    all_gather x3 -> x0, blocking collectives: 72.1 us -> none  [the longest x2 60.6 us: in_one_piece(): lax.all_gather(both, axis, axis=dim, tiled=True)]
    all_gather x3 -> x0, waiting for transfers between devices: 52.1 us -> none  [the longest x1 38.8 us: in_one_piece(): lax.all_gather(both, axis, axis=dim, tiled=True)]
    psum x2 -> x0, blocking collectives: 26.3 us -> none  [one_axis_at_a_time(): value = lax.psum(value, axis)]
    reduce_sum x18 -> x0, other arithmetic: 16.9 us -> none  [the longest x17 16.7 us: attend(): row_total = row_total * factor + jnp.sum(weights, axis=-1)]
    all_to_all x1 -> x0, blocking collectives: 10.8 us -> none  [per_device(): lax.all_to_all(gated, TP, split_axis=0, concat_axis=1, tiled=True)]
    unnamed x38 -> x2, local copies, waits for them, and re-layouts: 14 us -> 3.5 us
  transfers between devices with their start and end apart: 3 -> 0, of which waited for: 2 -> 0; matrix products, arithmetic and copies ran while one was open for 43% -> 0% of each run, Pallas kernels for 0% -> 0%
where the time goes in v1:
time: 81.3 us; the launch traced here: 81.2 us
  Pallas kernels  77.7 us (96%)
  local copies, waits for them, and re-layouts  3.5 us (4%)
    pallas_call x1, Pallas kernels, per_device(): pl.pallas_call(body, out_shape=jax.ShapeDtypeStruct((ROWS, WIDTH), BF16),...  77.7 us
    unnamed x2, local copies, waits for them, and re-layouts  3.5 us

profile of v1, /device:TPU:1, one launch (start us, length us, event | category | flops | bytes accessed | tf_op | source)
XLA Modules:
  0.0 81.2 jit_solution(10468275024314635762)
XLA Ops:
  0.0 1.9 %copy.23.rd_h = bf16[2048,32]{1,0:T(8,128)(2,1)} copy(bf16[2048,32]{0,1:T(8,128)(2,1)} %param.31) | data formatting | bytes 262144 | tf_op args[9]
  1.9 77.7 %shard_map.208 = bf16[40,2048]{1,0:T(8,128)(2,1)} custom-call(bf16[40,2048]{1,0:T(8,128)(2,1)} %lat_h.1, bf16[32,2048]{1,0:T(8,128)(2,1)} %ctx_h.1, f32[16,128]{1,0:T(8,128)} %bitcast.6, f32[16,128]{1,0:T(8,128)} %bitcast.7, bf16[64,256]{1,0:T(8,128)(2,1)} %shw_h.1, bf16[64,256]{1,0:T(8,128)(2,1)} %scw_h.1, bf16[64,256]{1,0:T(8,128)(2,1)} %mgw_h.1, ...), custom_call_target="tpu_custom_call" | custom-call | tf_op jit(solution)/shard_map/pallas_call | solution.py:438
  79.6 1.6 %copy.25 = bf16[40,2048]{1,0:T(8,128)(2,1)} copy(bf16[40,2048]{1,0:T(8,128)(2,1)} %shard_map.208) | data formatting | bytes 327680

commit v2 on v1

v2 whole, which is shorter than its diff:
```python
import math

import jax
import jax.numpy as jnp
import numpy as np
from jax import lax
from jax.experimental import pallas as pl
from jax.experimental.pallas import tpu as pltpu
from jax.sharding import PartitionSpec as P

F32, BF16 = jnp.float32, jnp.bfloat16
NZ, NY, NX, NC = 8, 4, 4, 2
NTP = NX * NC
NPLANE = NY * NTP
ROWS = 40
SLAB = 320
HALF = 160
CTXH = 16
PIECE = HALF + CTXH
MSG = PIECE + 32
CUT = 112
UNIT = 2 * NY * PIECE
WIDTH = 2048
COL = 256
EPS = 1e-06
OW_MID = 4
SQRT2 = 2.0**0.5
SCORE = math.log2(math.e) / math.sqrt(96.0)


def rope_tables():
    inverse = (10000.0 ** (-np.arange(8, dtype=np.float64) / 8)).astype(np.float32)
    lane = np.arange(128)
    axis, member, pair = (lane // 16) % 2, (lane // 8) % 2, lane % 8
    sign = np.where(member == 0, -1.0, 1.0)

    def rows_of(numbers, which):
        angle = (numbers[:, None].astype(np.float32) * inverse[pair][None, :]).astype(np.float64)
        keep = axis[None, :] == which
        return np.where(keep, np.cos(angle), 0.0), np.where(keep, np.sin(angle) * sign, 0.0)

    cos_row, sin_row = rows_of(np.arange(160), 0)
    cos_col, sin_col = rows_of(np.arange(64), 1)
    by_slab = np.zeros((32, 16, 128), np.float32)
    by_slab[:, 0:5] = cos_row.reshape(32, 5, 128)
    by_slab[:, 8:13] = sin_row.reshape(32, 5, 128)
    return by_slab, np.concatenate([cos_col, sin_col], 0).astype(np.float32)


def dot(a, b):
    return jnp.dot(a, b, preferred_element_type=F32)


def silu(v):
    return v / (1.0 + jnp.exp(-v))


def rms(v, gain):
    return v * lax.rsqrt(jnp.mean(v * v, axis=-1, keepdims=True) + EPS) * gain


def swap_members(v):
    lane = lax.broadcasted_iota(jnp.int32, v.shape, 1)
    return jnp.where(lane % 16 < 8, pltpu.roll(v, 120, 1), pltpu.roll(v, 8, 1))


def body(
    lat_h, ctx_h, cond_h, ctxv_h, shw_h, scw_h, mgw_h, qd_h, ld_h, rd_h, gw_h, qg_h, kg_h, qp_h, qr_h, ke_h, ve_h,
    ow_h, ng_h, nb_h, rrow_h, rcol_h, out,
    gath, ctx_v, cond_v, ctxv_v, w3, qd, ld, rd, gw, qg, kg, qp, qr, ke, ve, ow, ng, nb, rrow, rcol,
    zbuf, pbuf, gbuf, mod, xin, tabc, tabs, kv, ket, q2, kt2, acc, top, total, sgate, gsrc, gdst,
    lsem, zsend, zrecv, psend, precv, gsend, grecv, lx_send, lx_recv, kz_send, kz_recv, ky_send, ky_recv,
    kd_send, kd_recv, kf_send, kf_recv, ox_send, ox_recv, a_send, a_recv,
):
    sp, tp = lax.axis_index("sp"), lax.axis_index("tp")
    z, y, x, c = sp // NY, sp % NY, tp // NC, tp % NC

    def at_z(d):
        return {"sp": ((z + d) % NZ) * NY + y, "tp": tp}

    def at_y(d):
        return {"sp": z * NY + (y + d) % NY, "tp": tp}

    def slot_x(d):
        return ((x + d) % NX) * NC + c

    def at_x(d):
        return {"sp": sp, "tp": slot_x(d)}

    partner_slot = x * NC + (1 - c)
    partner = {"sp": sp, "tp": partner_slot}

    def at_tp(d):
        return {"sp": sp, "tp": (tp + d) % NTP}

    def push(src, dst, send, recv, to):
        pltpu.make_async_remote_copy(
            src_ref=src, dst_ref=dst, send_sem=send, recv_sem=recv, device_id=to, device_id_type=pl.DeviceIdType.MESH
        ).start()

    def take(ref, sem):
        pltpu.make_async_copy(ref, ref, sem).wait()

    local = [
        (cond_h, cond_v), (ctxv_h, ctxv_v), (shw_h, w3.at[0]), (scw_h, w3.at[1]), (mgw_h, w3.at[2]),
        (lat_h, gath.at[tp]), (ctx_h, ctx_v), (ld_h, ld), (rd_h, rd), (rrow_h.at[sp], rrow), (rcol_h, rcol),
        (kg_h, kg), (qd_h, qd), (qg_h, qg), (qp_h, qp), (qr_h, qr), (gw_h, gw), (ke_h, ke), (ve_h, ve),
        (ow_h, ow.at[tp]), (ng_h, ng), (nb_h, nb),
    ]
    for k, (src, dst) in enumerate(local):
        pltpu.make_async_copy(src, dst, lsem.at[k]).start()

    def have(*which):
        for k in which:
            take(local[k][1], lsem.at[k])

    barrier = pltpu.get_barrier_semaphore()
    plane = [(dy, dt) for dy in range(NY) for dt in range(NTP) if (dy, dt) != (0, 0)]

    def at_plane(dy, dt):
        return {"sp": z * NY + (y + dy) % NY, "tp": (tp + dt) % NTP}

    peers = [at_z(d) for d in range(1, NZ)] + [at_plane(dy, dt) for dy, dt in plane]
    for peer in peers:
        pl.semaphore_signal(barrier, inc=1, device_id=peer, device_id_type=pl.DeviceIdType.MESH)

    have(0, 1, 2, 3, 4)
    pick = pl.ds(sp // 2, 1)
    lane = lax.broadcasted_iota(jnp.int32, (8, 128), 1)
    line = lax.broadcasted_iota(jnp.int32, (8, 128), 0)
    mine = lane // 64 == sp % 2
    cond_row = jnp.broadcast_to(silu(cond_v[pick, :]), (8, 128))
    ctxv_row = jnp.broadcast_to(silu(ctxv_v[pick, :]), (8, 128))
    part = jnp.zeros((8, COL), F32)
    for k in range(3):
        at = 2 * k
        rows = jnp.where(line == at, cond_row, jnp.where(line == at + 1, ctxv_row, 0.0))
        rows = jnp.where(mine, rows, 0.0).astype(BF16)
        part = part + dot(rows, jnp.concatenate([w3[k], w3[k]], axis=0))
    zbuf[z] = jnp.concatenate([part[0:4, 0:128], part[0:4, 128:256], part[4:8, 0:128], part[4:8, 128:256]], axis=0)
    pl.semaphore_wait(barrier, len(peers))

    for d in range(1, NZ):
        push(zbuf.at[z], zbuf.at[z], zsend, zrecv, at_z(d))
    have(5)
    own = gath.at[tp]
    push(own, own, lx_send.at[0], lx_recv.at[0], at_x(1))
    push(own, own, lx_send.at[1], lx_recv.at[1], at_x(-1))
    push(own, own, lx_send.at[2], lx_recv.at[2], partner)
    take(zbuf.at[pl.ds(0, NZ - 1)], zrecv)
    whole = zbuf[0]
    for k in range(1, NZ):
        whole = whole + zbuf[k]
    me = y * NTP + tp
    pbuf[me] = whole[0:8]
    gbuf[me] = whole[8:16]
    for dy, dt in plane:
        push(pbuf.at[me], pbuf.at[me], psend, precv, at_plane(dy, dt))

    left, right, across = slot_x(-1), slot_x(1), slot_x(2)
    first, second = pl.ds(0, WIDTH // 2), pl.ds(WIDTH // 2, WIDTH // 2)
    take(gath.at[left], lx_recv.at[0])
    push(gath.at[left, :, first], gath.at[left, :, first], lx_send.at[3], lx_recv.at[3], at_x(1))
    push(gath.at[left], gath.at[left], lx_send.at[4], lx_recv.at[4], partner)
    take(gath.at[right], lx_recv.at[1])
    push(gath.at[right, :, second], gath.at[right, :, second], lx_send.at[5], lx_recv.at[5], at_x(-1))
    push(gath.at[right], gath.at[right], lx_send.at[6], lx_recv.at[6], partner)

    def gate_to_plane():
        for dy, dt in plane:
            push(gbuf.at[me], gbuf.at[me], gsend, grecv, at_plane(dy, dt))

    have(9, 10, 17)
    for k in range(5):
        rows = pl.ds(64 * k, 64)
        tabc[rows, :] = rrow[k : k + 1, :] + rcol[0:64, :]
        tabs[rows, :] = rrow[8 + k : 9 + k, :] + rcol[64:128, :]
    ket[...] = ke[...].astype(F32).T.astype(BF16)
    top[...] = jnp.full(top.shape, -1e30, F32)
    total[...] = jnp.zeros(total.shape, F32)
    acc[...] = jnp.zeros(acc.shape, F32)

    take(gath.at[across, :, first], lx_recv.at[3])
    take(gath.at[across, :, second], lx_recv.at[5])
    push(gath.at[across], gath.at[across], lx_send.at[7], lx_recv.at[7], partner)

    def from_plane(buf, sem):
        take(buf.at[pl.ds(0, NPLANE - 1)], sem)
        for t in range(NTP):
            mod[t] = (buf[t] + buf[NTP + t]) + (buf[2 * NTP + t] + buf[3 * NTP + t])

    from_plane(pbuf, precv)
    def vector(row):
        return jnp.concatenate([mod[t, r : r + 1, :] for t in range(NTP) for r in (row, row + 4)], axis=1)

    shift, scale = vector(0), 1.0 + vector(2)
    have(6, 7, 8, 11)
    lines = [gath[NC * k + c].astype(F32) for k in range(NX)]
    mine_lat = jnp.concatenate(lines, axis=0) * scale + shift
    mine_ctx = ctx_v[pl.ds(pl.multiple_of(CTXH * c, CTXH), CTXH), :].astype(F32) * (1.0 + vector(3)) + vector(1)
    mine_in = jnp.concatenate([mine_lat, mine_ctx], axis=0).astype(BF16)
    slot = NY * c + y
    kv[z, slot, 0:PIECE, :] = rms(dot(mine_in, ld[...]), kg[...]).astype(BF16)
    flat = lax.dot_general(mine_in, rd[...], (((1,), (1,)), ((), ())), preferred_element_type=F32)
    flat = jnp.concatenate([flat, jnp.zeros((PIECE, 96), F32)], axis=1)
    lat_part = flat[0:HALF]

    def rows_of(table):
        return jnp.concatenate(
            [table[pl.ds(pl.multiple_of(ROWS * (NC * k + c), 8), ROWS), :] for k in range(NX)], axis=0
        )

    turned = lat_part * rows_of(tabc) + swap_members(lat_part) * rows_of(tabs)
    both = jnp.concatenate([turned, flat[HALF:], jnp.zeros((256 - PIECE, 128), F32)], axis=0)
    kv[z, slot, PIECE:MSG, :] = both.T[0:32, :].astype(BF16)

    def z_of(i):
        off = (i % 2) * ((i + 1) // 2) - (1 - i % 2) * (i // 2)
        return (z + off + NZ) % NZ

    low, high = pl.ds(0, CUT), pl.ds(CUT, MSG - CUT)

    def z_back(i):
        return {"sp": ((z + NZ + 1 - 2 * (i % 2)) % NZ) * NY + y, "tp": tp}

    def at_slot(i, d):
        return kv.at[z_of(i), NY * c + (y + d + NY) % NY]

    def near_z(i):
        here = at_slot(i, 0)

        @pl.when(i < 7)
        def _():
            take(here, kz_recv.at[i, 0])

        @pl.when(i == 7)
        def _():
            take(here.at[low], kz_recv.at[7, 0])
            take(here.at[high], kz_recv.at[7, 1])

        @pl.when(i < 5)
        def _():
            push(here, here, kz_send.at[i + 2, 0], kz_recv.at[i + 2, 0], z_back(i))

        @pl.when(i == 5)
        def _():
            push(here.at[low], here.at[low], kz_send.at[7, 0], kz_recv.at[7, 0], at_z(-1))

        @pl.when(i == 6)
        def _():
            push(here.at[high], here.at[high], kz_send.at[7, 1], kz_recv.at[7, 1], at_z(1))

        to_y(i)

    def to_y(i):
        here = at_slot(i, 0)
        push(here, here, ky_send.at[i, 0], ky_recv.at[i, 0], at_y(1))
        push(here, here, ky_send.at[i, 1], ky_recv.at[i, 1], at_y(-1))

    def from_y(i):
        below, above = at_slot(i, -1), at_slot(i, 1)
        take(below, ky_recv.at[i, 0])
        push(below.at[low], below.at[low], ky_send.at[i, 2], ky_recv.at[i, 2], at_y(1))
        take(above, ky_recv.at[i, 1])
        push(above.at[high], above.at[high], ky_send.at[i, 3], ky_recv.at[i, 3], at_y(-1))

    def from_far(i):
        far = at_slot(i, 2)
        take(far.at[low], ky_recv.at[i, 2])
        take(far.at[high], ky_recv.at[i, 3])

    def to_partner(i):
        four = kv.at[z_of(i), pl.ds(NY * c, NY)]
        push(four, four, kd_send.at[i], kd_recv.at[i], partner)

    turn = (0, 1, -1, 2)

    def own_to_z(j):
        here = at_slot(0, turn[j])
        push(here, here, kz_send.at[1, j], kz_recv.at[1, j], at_z(-1))
        push(here, here, kz_send.at[2, j], kz_recv.at[2, j], at_z(1))

    def round_z(i):
        for j in range(4):
            here = at_slot(i, turn[j])
            take(here, kz_recv.at[i, j])

            @pl.when((i < 5) | ((i == 5) & (j < 2)) | ((i == 6) & (j >= 2)))
            def _(here=here, j=j):
                n = jnp.minimum(i + 2, 7)
                push(here, here, kz_send.at[n, j], kz_recv.at[n, j], z_back(i))

    first_y = kv.at[z, slot]
    push(first_y.at[low], first_y.at[low], kf_send.at[0], kf_recv.at[0], at_y(1))
    push(first_y.at[high], first_y.at[high], kf_send.at[1], kf_recv.at[1], at_y(-1))
    push(first_y.at[high], first_y.at[high], kf_send.at[2], kf_recv.at[2], at_y(1))
    push(first_y.at[low], first_y.at[low], kf_send.at[3], kf_recv.at[3], at_y(-1))
    own_to_z(0)
    have(19)
    owned = ow.at[tp]
    push(owned, owned, ox_send.at[0], ox_recv.at[0], at_x(1))
    push(owned, owned, ox_send.at[1], ox_recv.at[1], at_x(-1))
    push(owned, owned, ox_send.at[2], ox_recv.at[2], partner)

    take(gath.at[partner_slot], lx_recv.at[2])
    for n, d in ((4, -1), (6, 1), (7, 2)):
        take(gath.at[((x + d) % NX) * NC + (1 - c)], lx_recv.at[n])
    for p in range(NTP // 2):
        pair = jnp.concatenate([gath[2 * p].astype(F32), gath[2 * p + 1].astype(F32)], axis=0)
        xin[2 * ROWS * p : 2 * ROWS * (p + 1), :] = (pair * scale + shift).astype(BF16)

    have(12, 13, 14, 15)
    q_codes = rms(dot(xin[...], qd[...]), qg[...]).astype(BF16)
    q_cont = dot(q_codes, qp[...]) * SCORE
    q_rot = dot(q_codes, qr[...])
    q_rot = (q_rot * tabc[...] + swap_members(q_rot) * tabs[...]) * SCORE
    q_lane = lax.broadcasted_iota(jnp.int32, (SLAB, 128), 1)
    for h in range(4):
        j, rows = h // 2, pl.ds(SLAB * (h % 2), SLAB)
        plain = q_cont[:, 128 * j : 128 * (j + 1)]
        q2[j, rows, 0:128] = jnp.where(q_lane // 64 == h % 2, plain, 0.0).astype(BF16)
        q2[j, rows, 128:256] = jnp.where(q_lane // 32 == h, q_rot, 0.0).astype(BF16)
    below, above = at_slot(0, -1), at_slot(0, 1)
    take(below.at[low], kf_recv.at[0])
    push(below.at[low], below.at[low], ky_send.at[0, 2], ky_recv.at[0, 2], at_y(1))
    take(above.at[high], kf_recv.at[1])
    push(above.at[high], above.at[high], ky_send.at[0, 3], ky_recv.at[0, 3], at_y(-1))

    @pl.when(c == 0)
    def _():
        near_z(1)
        near_z(2)

    take(below.at[high], kf_recv.at[2])
    take(above.at[low], kf_recv.at[3])

    @pl.when(c == 1)
    def _():
        own_to_z(1)
        own_to_z(2)

    have(16)
    sgate[...] = silu(dot(xin[...], gw[...]).astype(BF16).astype(F32))
    from_far(0)
    to_partner(0)

    @pl.when(c == 0)
    def _():
        from_y(1)

    @pl.when(c == 1)
    def _():
        own_to_z(3)

    def halfway(i):
        @pl.when((c == 1) & (i % 2 == 0))
        def _():
            round_z(i + 1)

        @pl.when((c == 1) & (i % 2 == 0) & (i < 6))
        def _():
            round_z(i + 2)

        @pl.when((c == 0) & (i < 7))
        def _():
            from_far(i + 1)

        @pl.when(i < 7)
        def _():
            to_partner(i + 1)

    def one_unit(i, carry):
        @pl.when((c == 0) & (i < 5))
        def _():
            near_z(i + 3)

        @pl.when((c == 0) & (i < 6))
        def _():
            from_y(i + 2)

        @pl.when(i == 1)
        def _():
            gate_to_plane()

        @pl.when(i == OW_MID)
        def _():
            take(ow.at[left], ox_recv.at[0])
            push(ow.at[left, pl.ds(0, 128)], ow.at[left, pl.ds(0, 128)], ox_send.at[3], ox_recv.at[3], at_x(1))
            push(ow.at[left], ow.at[left], ox_send.at[4], ox_recv.at[4], partner)
            take(ow.at[right], ox_recv.at[1])
            push(ow.at[right, pl.ds(128, 128)], ow.at[right, pl.ds(128, 128)], ox_send.at[5], ox_recv.at[5], at_x(-1))
            push(ow.at[right], ow.at[right], ox_send.at[6], ox_recv.at[6], partner)

        @pl.when(i == 7)
        def _():
            take(ow.at[across, pl.ds(0, 128)], ox_recv.at[3])
            take(ow.at[across, pl.ds(128, 128)], ox_recv.at[5])
            push(ow.at[across], ow.at[across], ox_send.at[7], ox_recv.at[7], partner)

        at = z_of(i)
        take(kv.at[at, pl.ds(NY * (1 - c), NY)], kd_recv.at[i])
        codes = jnp.concatenate([kv[at, p, 0:PIECE, :] for p in range(2 * NY)], axis=0)
        rot = jnp.concatenate([kv[at, p, PIECE:MSG, 0:PIECE] for p in range(2 * NY)], axis=1)
        keys = lax.dot_general(ket[...], codes, (((1,), (1,)), ((), ())), preferred_element_type=F32).astype(BF16)
        for j in range(2):
            kt2[j, 0:128, :] = keys[128 * j : 128 * (j + 1)]
            for h in range(4):
                kt2[j, 128 + 32 * h : 160 + 32 * h, :] = rot

        def scores(h):
            return dot(q2[h // 2, SLAB * (h % 2) : SLAB * (h % 2 + 1), :], kt2[h // 2])

        coming = scores(0)
        for h in range(4):
            s = coming
            if h == 2:
                halfway(i)
            if h < 3:
                coming = scores(h + 1)
            rows = pl.ds(SLAB * h, SLAB)
            old = top[rows, :]
            new = jnp.maximum(old, jnp.max(s, axis=1, keepdims=True))
            w = jnp.exp2(s - new)
            fade = jnp.exp2(old - new)
            top[rows, :] = new
            total[rows, :] = total[rows, :] * fade + jnp.sum(w, axis=1, keepdims=True)
            acc[rows, :] = acc[rows, :] * fade + dot(w.astype(BF16), codes)
        return carry

    lax.fori_loop(0, NZ, one_unit, 0)

    have(18)
    col = lax.broadcasted_iota(jnp.int32, (SLAB, COL), 1)
    attended = jnp.zeros((SLAB, COL), F32)
    for h in range(4):
        rows = pl.ds(SLAB * h, SLAB)
        inner = (acc[rows, :] / total[rows, :]).astype(BF16)
        attended = jnp.where(col // 64 == h, dot(inner, ve[...]), attended)
    gated = attended * sgate[...]
    for t in range(NTP):
        gsrc[t] = gated[ROWS * t : ROWS * (t + 1), :].astype(BF16)
    gdst[tp] = gsrc[tp]
    sources = (1, 7, 2, 6, 3, 5, 4)
    for n, d in enumerate(sources):
        push(gsrc.at[(tp + d) % NTP], gdst.at[tp], a_send, a_recv.at[n], at_tp(d))

    have(20, 21)
    from_plane(gbuf, grecv)
    take(zbuf.at[pl.ds(0, NZ - 1)], zsend)
    take(pbuf.at[pl.ds(0, NPLANE - 1)], psend)
    take(gbuf.at[pl.ds(0, NPLANE - 1)], gsend)
    for n in (0, 1, 2, 4, 6, 7):
        take(gath.at[tp], lx_send.at[n])
        take(ow.at[tp], ox_send.at[n])
    for n in (3, 5):
        take(gath.at[tp, :, first], lx_send.at[n])
        take(ow.at[tp, pl.ds(0, 128)], ox_send.at[n])
    here = kv.at[z, slot]

    def sent_along_y(i):
        take(here, ky_send.at[i, 0])
        take(here, ky_send.at[i, 1])
        take(here.at[low], ky_send.at[i, 2])
        take(here.at[high], ky_send.at[i, 3])

    take(here.at[low], kf_send.at[0])
    take(here.at[high], kf_send.at[1])
    take(here.at[high], kf_send.at[2])
    take(here.at[low], kf_send.at[3])
    take(here.at[low], ky_send.at[0, 2])
    take(here.at[high], ky_send.at[0, 3])
    take(kv.at[z, pl.ds(0, NY)], kd_send.at[0])

    def drain(i, carry):
        take(kv.at[z, pl.ds(0, NY)], kd_send.at[i])

        @pl.when(c == 0)
        def _():
            sent_along_y(i)

        @pl.when((c == 1) | (i < 7))
        def _():
            take(here, kz_send.at[i, 0])

        @pl.when(c == 1)
        def _():
            for j in range(1, 4):
                take(here, kz_send.at[i, j])

        return carry

    lax.fori_loop(1, NZ, drain, 0)

    @pl.when(c == 0)
    def _():
        take(here.at[low], kz_send.at[7, 0])
        take(here.at[high], kz_send.at[7, 1])

    take(ow.at[partner_slot], ox_recv.at[2])
    for n, d in ((4, -1), (6, 1), (7, 2)):
        take(ow.at[((x + d) % NX) * NC + (1 - c)], ox_recv.at[n])
    outer = dot(gdst[tp], ow[tp])
    for n, d in enumerate(sources):
        src = (tp - d) % NTP
        take(gdst.at[src], a_recv.at[n])
        outer = outer + dot(gdst[src], ow[src])
    blended = SQRT2 * gath[tp].astype(F32) + vector(0) * outer
    centred = blended - jnp.mean(blended, axis=-1, keepdims=True)
    spread = jnp.mean(centred * centred, axis=-1, keepdims=True)
    out[...] = (centred * lax.rsqrt(spread + EPS) * ng[...] + nb[...]).astype(BF16)
    take(gsrc.at[pl.ds(0, NTP - 1)], a_send)


def per_device(
    latents, context, cond_vec, ctx_vec, shift_w, scale_w, modgate_w, query_down_weight, latent_down_weight, rot_down,
    gate_w, query_norm_gain, latent_norm_gain, query_plain_weight, query_rotary_weight, key_expand_weight,
    value_expand_weight, out_w, norm_gain, norm_bias,
):
    by_slab, by_col = rope_tables()
    args = (
        latents, context, cond_vec.reshape(16, 128), ctx_vec.reshape(16, 128), shift_w, scale_w, modgate_w,
        query_down_weight, latent_down_weight, rot_down.T, gate_w, query_norm_gain.reshape(1, 512),
        latent_norm_gain.reshape(1, COL), query_plain_weight, query_rotary_weight, key_expand_weight,
        value_expand_weight, out_w, norm_gain.reshape(1, WIDTH), norm_bias.reshape(1, WIDTH),
        jnp.asarray(by_slab), jnp.asarray(by_col),
    )
    vm = pltpu.VMEM
    dma = pltpu.SemaphoreType.DMA
    scratch = [
        vm((NTP, ROWS, WIDTH), BF16), vm((32, WIDTH), BF16), vm((16, 128), F32), vm((16, 128), F32),
        vm((3, 64, COL), BF16), vm((WIDTH, 512), BF16), vm((WIDTH, COL), BF16), vm((32, WIDTH), BF16),
        vm((WIDTH, COL), BF16), vm((1, 512), F32), vm((1, COL), F32), vm((512, COL), BF16), vm((512, 128), BF16),
        vm((COL, COL), BF16), vm((COL, COL), BF16), vm((NTP, COL, WIDTH), BF16), vm((1, WIDTH), F32),
        vm((1, WIDTH), F32), vm((16, 128), F32), vm((128, 128), F32),
        vm((NZ, 16, 128), F32), vm((NPLANE, 8, 128), F32), vm((NPLANE, 8, 128), F32), vm((NTP, 8, 128), F32),
        vm((SLAB, WIDTH), BF16),
        vm((SLAB, 128), F32), vm((SLAB, 128), F32), vm((NZ, 2 * NY, MSG, COL), BF16),
        vm((COL, COL), BF16), vm((2, 2 * SLAB, COL), BF16), vm((2, COL, UNIT), BF16), vm((4 * SLAB, COL), F32),
        vm((4 * SLAB, 1), F32), vm((4 * SLAB, 1), F32), vm((SLAB, COL), F32), vm((NTP, ROWS, COL), BF16),
        vm((NTP, ROWS, COL), BF16),
        dma((22,)), dma, dma, dma, dma, dma, dma,
        dma((8,)), dma((8,)), dma((NZ, 4)), dma((NZ, 4)), dma((NZ, 4)), dma((NZ, 4)), dma((NZ,)), dma((NZ,)), dma((4,)), dma((4,)),
        dma((8,)), dma((8,)), dma, dma((NTP - 1,)),
    ]
    return pl.pallas_call(
        body,
        out_shape=jax.ShapeDtypeStruct((ROWS, WIDTH), BF16),
        in_specs=[pl.BlockSpec(memory_space=pl.ANY)] * len(args),
        out_specs=pl.BlockSpec(memory_space=pltpu.VMEM),
        scratch_shapes=scratch,
        compiler_params=pltpu.CompilerParams(collective_id=0, has_side_effects=True, vmem_limit_bytes=62 * 1024 * 1024),
    )(*args)


def solution(mesh):
    tp, sp = P(None, "tp"), P("sp", "tp")
    return jax.shard_map(
        per_device,
        mesh=mesh,
        in_specs=(
            P(("sp", "tp"), None), P("sp", None), P(), P(), sp, sp, sp, P(), P(), P(), tp, P(), P(), tp, tp, tp, tp,
            P("tp", None), P(), P(),
        ),
        out_specs=P(("sp", "tp"), None),
        check_vma=False,
    )
```

time: 81.3 us -> 75.2 us (0.925)
  Pallas kernels: 77.7 us -> 73.5 us
  local copies, waits for them, and re-layouts: 3.5 us -> 1.59 us
    pallas_call x1, Pallas kernels: 77.7 us -> 73.5 us  [per_device(): pl.pallas_call(body, out_shape=jax.ShapeDtypeStruct((ROWS, WIDTH), BF16),...]
    unnamed x2 -> x1, local copies, waits for them, and re-layouts: 3.5 us -> 1.59 us
where the time goes in v2:
time: 75.2 us; the launch traced here: 75.1 us
  Pallas kernels  73.5 us (98%)
  local copies, waits for them, and re-layouts  1.59 us (2%)
    pallas_call x1, Pallas kernels, per_device(): pl.pallas_call(body, out_shape=jax.ShapeDtypeStruct((ROWS, WIDTH), BF16),...  73.5 us
    unnamed x1, local copies, waits for them, and re-layouts  1.59 us

profile of v2, /device:TPU:1, one launch (start us, length us, event | category | flops | bytes accessed | tf_op | source)
XLA Modules:
  0.0 75.1 jit_solution(4568369812686989335)
XLA Ops:
  0.0 73.5 %shard_map.208 = bf16[40,2048]{1,0:T(8,128)(2,1)} custom-call(bf16[40,2048]{1,0:T(8,128)(2,1)} %lat_h.1, bf16[32,2048]{1,0:T(8,128)(2,1)} %ctx_h.1, f32[16,128]{1,0:T(8,128)} %bitcast.8, f32[16,128]{1,0:T(8,128)} %bitcast.9, bf16[64,256]{1,0:T(8,128)(2,1)} %shw_h.1, bf16[64,256]{1,0:T(8,128)(2,1)} %scw_h.1, bf16[64,256]{1,0:T(8,128)(2,1)} %mgw_h.1, ...), custom_call_target="tpu_custom_call" | custom-call | tf_op jit(solution)/shard_map/pallas_call | solution.py:545
  73.5 1.6 %copy.24 = bf16[40,2048]{1,0:T(8,128)(2,1)} copy(bf16[40,2048]{1,0:T(8,128)(2,1)} %shard_map.208) | data formatting | bytes 327680

commit v3 on v2

--- a/solution.py
+++ b/solution.py
@@ -544,7 +544,7 @@
     ]
     return pl.pallas_call(
         body,
-        out_shape=jax.ShapeDtypeStruct((ROWS, WIDTH), BF16),
+        out_shape=pltpu.VMEM((ROWS, WIDTH), BF16),
         in_specs=[pl.BlockSpec(memory_space=pl.ANY)] * len(args),
         out_specs=pl.BlockSpec(memory_space=pltpu.VMEM),
         scratch_shapes=scratch,

time: 75.2 us -> 73.7 us (0.980)
  local copies, waits for them, and re-layouts: 1.59 us -> 0.67 us
    unnamed x1, local copies, waits for them, and re-layouts: 1.59 us -> 0.67 us
where the time goes in v3:
time: 73.7 us; the launch traced here: 73.5 us
  Pallas kernels  72.9 us (99%)
    pallas_call x1, Pallas kernels, per_device(): pl.pallas_call(body, out_shape=pltpu.VMEM((ROWS, WIDTH), BF16), in_specs=...  72.9 us

profile of v3, /device:TPU:1, one launch (start us, length us, event | category | flops | bytes accessed | tf_op | source)
XLA Modules:
  0.0 73.5 jit_solution(17040470657335498103)
XLA Ops:
  0.0 72.9 %shard_map.208 = bf16[40,2048]{1,0:T(8,128)(2,1)S(1)} custom-call(bf16[40,2048]{1,0:T(8,128)(2,1)} %lat_h.1, bf16[32,2048]{1,0:T(8,128)(2,1)} %ctx_h.1, f32[16,128]{1,0:T(8,128)} %bitcast.8, f32[16,128]{1,0:T(8,128)} %bitcast.9, bf16[64,256]{1,0:T(8,128)(2,1)} %shw_h.1, bf16[64,256]{1,0:T(8,128)(2,1)} %scw_h.1, bf16[64,256]{1,0:T(8,128)(2,1)} %mgw_h.1, ...), custom_call_target="tpu_custom_call" | custom-call | tf_op jit(solution)/shard_map/pallas_call | solution.py:545
  72.9 0.7 copy.24

commit v4 on v3

--- a/solution.py
+++ b/solution.py
@@ -116,6 +116,7 @@
 
     barrier = pltpu.get_barrier_semaphore()
     plane = [(dy, dt) for dy in range(NY) for dt in range(NTP) if (dy, dt) != (0, 0)]
+    plane.sort(key=lambda at: -min(at[0], NY - at[0]) - min(at[1], NTP - at[1]) / 2)
 
     def at_plane(dy, dt):
         return {"sp": z * NY + (y + dy) % NY, "tp": (tp + dt) % NTP}
@@ -140,13 +141,22 @@
     zbuf[z] = jnp.concatenate([part[0:4, 0:128], part[0:4, 128:256], part[4:8, 0:128], part[4:8, 128:256]], axis=0)
     pl.semaphore_wait(barrier, len(peers))
 
-    for d in range(1, NZ):
+    for d in (4, 3, 5, 2, 6, 1, 7):
         push(zbuf.at[z], zbuf.at[z], zsend, zrecv, at_z(d))
     have(5)
     own = gath.at[tp]
     push(own, own, lx_send.at[0], lx_recv.at[0], at_x(1))
     push(own, own, lx_send.at[1], lx_recv.at[1], at_x(-1))
     push(own, own, lx_send.at[2], lx_recv.at[2], partner)
+    left, right, across = slot_x(-1), slot_x(1), slot_x(2)
+    first, second = pl.ds(0, WIDTH // 2), pl.ds(WIDTH // 2, WIDTH // 2)
+    take(gath.at[left], lx_recv.at[0])
+    push(gath.at[left, :, first], gath.at[left, :, first], lx_send.at[3], lx_recv.at[3], at_x(1))
+    push(gath.at[left], gath.at[left], lx_send.at[4], lx_recv.at[4], partner)
+    take(gath.at[right], lx_recv.at[1])
+    push(gath.at[right, :, second], gath.at[right, :, second], lx_send.at[5], lx_recv.at[5], at_x(-1))
+    push(gath.at[right], gath.at[right], lx_send.at[6], lx_recv.at[6], partner)
+
     take(zbuf.at[pl.ds(0, NZ - 1)], zrecv)
     whole = zbuf[0]
     for k in range(1, NZ):
@@ -156,15 +166,6 @@
     gbuf[me] = whole[8:16]
     for dy, dt in plane:
         push(pbuf.at[me], pbuf.at[me], psend, precv, at_plane(dy, dt))
-
-    left, right, across = slot_x(-1), slot_x(1), slot_x(2)
-    first, second = pl.ds(0, WIDTH // 2), pl.ds(WIDTH // 2, WIDTH // 2)
-    take(gath.at[left], lx_recv.at[0])
-    push(gath.at[left, :, first], gath.at[left, :, first], lx_send.at[3], lx_recv.at[3], at_x(1))
-    push(gath.at[left], gath.at[left], lx_send.at[4], lx_recv.at[4], partner)
-    take(gath.at[right], lx_recv.at[1])
-    push(gath.at[right, :, second], gath.at[right, :, second], lx_send.at[5], lx_recv.at[5], at_x(-1))
-    push(gath.at[right], gath.at[right], lx_send.at[6], lx_recv.at[6], partner)
 
     def gate_to_plane():
         for dy, dt in plane:

time: 73.7 us -> 74.1 us (level)
  no operation moved by 1% of the time
where the time goes in v4:
time: 74.1 us; the launch traced here: 74 us
  Pallas kernels  73.3 us (99%)
    pallas_call x1, Pallas kernels, per_device(): pl.pallas_call(body, out_shape=pltpu.VMEM((ROWS, WIDTH), BF16), in_specs=...  73.3 us

profile of v4, /device:TPU:1, one launch (start us, length us, event | category | flops | bytes accessed | tf_op | source)
XLA Modules:
  0.0 74.0 jit_solution(14303324517699302064)
XLA Ops:
  0.0 73.3 %shard_map.208 = bf16[40,2048]{1,0:T(8,128)(2,1)S(1)} custom-call(bf16[40,2048]{1,0:T(8,128)(2,1)} %lat_h.1, bf16[32,2048]{1,0:T(8,128)(2,1)} %ctx_h.1, f32[16,128]{1,0:T(8,128)} %bitcast.8, f32[16,128]{1,0:T(8,128)} %bitcast.9, bf16[64,256]{1,0:T(8,128)(2,1)} %shw_h.1, bf16[64,256]{1,0:T(8,128)(2,1)} %scw_h.1, bf16[64,256]{1,0:T(8,128)(2,1)} %mgw_h.1, ...), custom_call_target="tpu_custom_call" | custom-call | tf_op jit(solution)/shard_map/pallas_call | solution.py:546
  73.3 0.7 copy.24
